TPU v7x, 32 devices: a whole 2x2x4 slice. The times are simulated.
32 devices in a mesh: grp: 2 (over y), sp: 4 (over z), tp: 4 (over x, core).
Axes of the slice: x: 2, y: 2, z: 4, core: 2. Of those that a mesh axis runs over, the one named last changes fastest.
Arguments:
- recept: bfloat16 [4096, 2048], P(('grp', 'sp'), 'tp'), parts along dimension 0, may hold values from -6 to 6
- key_input: bfloat16 [4096, 2048], P(('grp', 'sp'), 'tp'), parts along dimension 0, may hold values from -6 to 6
- value_input: bfloat16 [4096, 2048], P(('grp', 'sp'), 'tp'), parts along dimension 0, may hold values from -6 to 6
- output_gate_input: bfloat16 [4096, 2048], P(('grp', 'sp'), 'tp'), parts along dimension 0, may hold values from -6 to 6
- decay_input_part: bfloat16 [4096, 2048], P(('grp', 'sp'), 'tp'), parts along dimension 0, may hold values from -4.8 to 4.8
- correction_rate_input: bfloat16 [4096, 2048], P(('grp', 'sp'), 'tp'), parts along dimension 0, may hold values from -4 to 4
- head_decay_offset: float32 [4096, 32], P(('grp', 'sp'), 'tp'), parts along dimension 0, may hold values from -2.1 to 0
- decay_fixed_bias: float32 [2048], P('tp'), may hold values from -11.5 to -2.8
- correction_rate_bias: float32 [2048], P('tp'), may hold values from -8.5 to 1
- head_norm_gain: float32 [2048], P('tp'), may hold values from 0.1 to 1.9
- self_term_weight: float32 [2048], P('tp'), may hold values from -2 to 2
- output_weight_matrix: bfloat16 [2048, 2048], P('tp'), may hold values from -0.125 to 0.125
- residual: bfloat16 [4096, 2048], P(('grp', 'sp', 'tp')), parts along dimension 0, may hold values from -6 to 6
- feedforward_norm_gain: float32 [2048], replicated, may hold values from 0.1 to 1.9
- routed_expert_index: int32 [4096, 2], P(('grp', 'sp', 'tp')), parts along dimension 0, may hold values from 0 to 3, all different within a row; in each aligned block of 128 rows (0 to 127, 128 to 255, ...) at most 96 rows name the same one
- routed_expert_weight: float32 [4096, 2], P(('grp', 'sp', 'tp')), parts along dimension 0, may hold values from 0.2 to 1
- gate_weight_experts: bfloat16 [4, 2048, 1024], P('sp', None, 'tp'), may hold values from -0.125 to 0.125
- up_weight_experts: bfloat16 [4, 2048, 1024], P('sp', None, 'tp'), may hold values from -0.125 to 0.125
- down_weight_experts: bfloat16 [4, 1024, 2048], P('sp', 'tp'), may hold values from -0.1875 to 0.1875
Outputs:
- output: bfloat16 [4096, 2048], P(('grp', 'sp', 'tp')), parts along dimension 0
There are 2 independent parts, one for each index of `grp`. A program takes and returns all parts, laid end to end along the dimension named above; an argument that names none is the same for every part. Nothing has to cross between parts.
Inputs may be any that keep to these rules, and one draw needn't show every extreme that they name: `routed_expert_index`: in each aligned block of 128 rows (the rows of one device) no expert is named by more than 96 routes; the two experts of a row differ.
All inputs are finite; a program needn't handle non-finite values.
Results may differ from a plain program's by a relative error of at most 0.0058.
Values may be sent and summed in bfloat16 or wider, within the bound.
A program may use at most 128 MiB of HBM per device.

v0:
```python
import jax
import jax.numpy as jnp
from jax import lax
from jax.sharding import PartitionSpec as P

SPAN = 64


PRECISE = lax.Precision.HIGHEST
GROUP_EPS = 0.00064
NORM_EPS = 1e-06


def prefix_2(part, axis, combine, identity):
    place = lax.axis_index(axis)
    gathered = jax.tree.map(lambda a: lax.all_gather(a, axis), part)
    state = jax.tree.map(lambda a, e: jnp.zeros_like(a) + jnp.asarray(e, a.dtype), part, identity)

    def one(lap, state):
        return combine(
            state, jax.tree.map(lambda a: lax.dynamic_index_in_dim(a, lap, 0, False), gathered)
        )

    return lax.fori_loop(0, place, one, state)


def chain_combine(earlier, later):
    transit = jnp.einsum("hij,hjk->hik", earlier[0], later[0], precision=PRECISE)
    carried = jnp.einsum("hij,hjk->hik", earlier[1], later[0], precision=PRECISE) + later[1]
    return (transit, carried)


def pair_scores(left, right):
    return jnp.einsum("bhtn,bhsn->bhts", left, right, precision=PRECISE)


def apply_scores(left, right):
    return jnp.einsum("bhts,bhsn->bhtn", left, right, precision=PRECISE)


def outer_sum(left, right):
    return jnp.einsum("bhtn,bhtm->bhnm", left, right, precision=PRECISE)


def square_blocks(left, right):
    return jnp.einsum("bhts,bhsu->bhtu", left, right, precision=PRECISE)


def unit_lower_inverse(strict_lower, span):
    inverse = jnp.eye(span, dtype=jnp.float32) + strict_lower
    power = strict_lower
    for level in range(1, (span - 1).bit_length()):
        power = square_blocks(power, power)
        inverse = inverse + square_blocks(power, inverse)
    return inverse


def mixer(
    recept,
    key_input,
    value_input,
    output_gate_input,
    decay_input_part,
    correction_rate_input,
    head_decay_offset,
    decay_fixed_bias,
    correction_rate_bias,
    head_norm_gain,
    self_term_weight,
    span,
):
    sequence_length, channel_width = recept.shape
    head_split = head_decay_offset.shape[1]
    head_width = channel_width // head_split
    blocks = sequence_length // span

    def split_heads(tensor):
        return (
            tensor.astype(jnp.float32)
            .reshape(blocks, span, head_split, head_width)
            .transpose(0, 2, 1, 3)
        )

    weight_logarithm = (
        -jax.nn.softplus(-(decay_fixed_bias + decay_input_part.astype(jnp.float32))) - 0.5
    )
    decay_logarithm = (
        -jnp.exp(weight_logarithm).reshape(sequence_length, head_split, head_width)
        + head_decay_offset[:, :, None]
    )
    decay_logarithm = split_heads(decay_logarithm.reshape(sequence_length, channel_width))
    rate = split_heads(
        jax.nn.sigmoid(correction_rate_bias + correction_rate_input.astype(jnp.float32))
    )
    receptance_per_head, key_per_head, value_per_head = (
        split_heads(recept),
        split_heads(key_input),
        split_heads(value_input),
    )
    unit_key = key_per_head * lax.rsqrt(
        jnp.sum(key_per_head * key_per_head, axis=-1, keepdims=True) + NORM_EPS
    )
    remove_vec = -unit_key
    write_vec = unit_key * rate
    cumul = jnp.cumsum(decay_logarithm, axis=2)
    remove_til = remove_vec * jnp.exp(cumul - decay_logarithm)
    recept_til = receptance_per_head * jnp.exp(cumul)
    write_hat = write_vec * jnp.exp(-cumul)
    key_hat = key_per_head * jnp.exp(-cumul)
    ending = jnp.exp(cumul[:, :, -1:, :])
    offsets = jnp.arange(span, dtype=jnp.int32)
    strict = offsets[:, None] > offsets[None, :]
    within = offsets[:, None] >= offsets[None, :]
    remove_write = jnp.where(strict, pair_scores(remove_til, write_hat), 0.0)
    remove_key = jnp.where(strict, pair_scores(remove_til, key_hat), 0.0)
    read_write = jnp.where(within, pair_scores(recept_til, write_hat), 0.0)
    read_key = jnp.where(within, pair_scores(recept_til, key_hat), 0.0)
    inverse = unit_lower_inverse(remove_write, span)
    inv_remove = apply_scores(inverse, remove_til)
    inv_value = apply_scores(inverse, apply_scores(remove_key, value_per_head))
    read_map = recept_til + apply_scores(read_write, inv_remove)
    read_own = apply_scores(read_write, inv_value) + apply_scores(read_key, value_per_head)
    write_end = write_hat * ending
    key_end = key_hat * ending
    eye_head = jnp.eye(head_width, dtype=jnp.float32)
    transit = outer_sum(inv_remove, write_end) + eye_head * ending[:, :, 0, None, :]
    added = outer_sum(inv_value, write_end) + outer_sum(value_per_head, key_end)
    identity = jnp.broadcast_to(eye_head, (head_split, head_width, head_width))
    zero_state = jnp.zeros((head_split, head_width, head_width), jnp.float32)

    def block_step(carry, inputs):
        return (chain_combine(carry, inputs), carry)

    device_total, block_starts = lax.scan(block_step, (identity, zero_state), (transit, added))
    prefix = prefix_2(device_total, "sp", chain_combine, (identity, zero_state))
    entering = prefix[1]
    true_start = (
        jnp.einsum("hvk,bhkm->bhvm", entering, block_starts[0], precision=PRECISE) + block_starts[1]
    )
    readout = jnp.einsum("bhtk,bhvk->bhtv", read_map, true_start, precision=PRECISE) + read_own
    center = jnp.mean(readout, axis=-1, keepdims=True)
    spread = jnp.mean(jnp.square(readout - center), axis=-1, keepdims=True)
    gains = head_norm_gain.reshape(head_split, head_width)[None, :, None, :]
    normalized_state = (readout - center) * lax.rsqrt(spread + GROUP_EPS) * gains
    self_term_head = self_term_weight.reshape(head_split, head_width)[None, :, None, :]
    self_term = (
        jnp.sum(receptance_per_head * key_per_head * self_term_head, axis=-1, keepdims=True)
        * value_per_head
    )
    merged_heads = (
        (normalized_state + self_term).transpose(0, 2, 1, 3).reshape(sequence_length, channel_width)
    )
    return (merged_heads * output_gate_input.astype(jnp.float32)).astype(jnp.bfloat16)


def local(
    recept,
    key_input,
    value_input,
    output_gate_input,
    decay_input_part,
    correction_rate_input,
    head_decay_offset,
    decay_fixed_bias,
    correction_rate_bias,
    head_norm_gain,
    self_term_weight,
    output_weight_matrix,
    residual,
    feedforward_norm_gain,
    routed_expert_index,
    routed_expert_weight,
    gate_weight_experts,
    up_weight_experts,
    down_weight_experts,
):
    attention_result = mixer(
        recept,
        key_input,
        value_input,
        output_gate_input,
        decay_input_part,
        correction_rate_input,
        head_decay_offset,
        decay_fixed_bias,
        correction_rate_bias,
        head_norm_gain,
        self_term_weight,
        SPAN,
    )
    proj = lax.psum_scatter(
        jnp.dot(attention_result, output_weight_matrix, preferred_element_type=jnp.float32),
        "tp",
        scatter_dimension=0,
        tiled=True,
    )
    proj = proj.astype(jnp.bfloat16)
    stream = residual.astype(jnp.float32) + lax.optimization_barrier(proj).astype(jnp.float32)
    ffn_in = (
        stream
        * lax.rsqrt(jnp.mean(stream * stream, axis=-1, keepdims=True) + NORM_EPS)
        * feedforward_norm_gain
    ).astype(jnp.bfloat16)
    local_rows = ffn_in.shape[0]
    top_count = routed_expert_index.shape[1]
    experts = gate_weight_experts.shape[0] * lax.axis_size("sp")
    capacity = max(2, 3 * local_rows // experts)
    flat_ids = routed_expert_index.reshape(-1)
    hits = (flat_ids[:, None] == jnp.arange(experts, dtype=jnp.int32)[None, :]).astype(jnp.int32)
    earlier_hits = jnp.cumsum(hits, axis=0) - hits
    slot_index = jnp.sum(earlier_hits * hits, axis=1)
    target = flat_ids * capacity + slot_index
    places = (target[:, None] == jnp.arange(experts * capacity, dtype=jnp.int32)[None, :]).astype(
        jnp.bfloat16
    )
    places = jnp.sum(places.reshape(local_rows, top_count, experts * capacity), axis=1)
    outgoing = jnp.einsum("rs,rd->sd", places, ffn_in, preferred_element_type=jnp.float32)
    outgoing = outgoing.astype(jnp.bfloat16).reshape(experts, capacity, ffn_in.shape[1])
    incoming = lax.all_gather(
        lax.all_to_all(outgoing, "sp", split_axis=0, concat_axis=0, tiled=True),
        "tp",
        axis=0,
        tiled=True,
    )
    flat = incoming.reshape(-1, incoming.shape[-1])
    gated = jnp.dot(flat, gate_weight_experts[0], preferred_element_type=jnp.float32)
    upward = jnp.dot(flat, up_weight_experts[0], preferred_element_type=jnp.float32)
    hidden = (jax.nn.silu(gated) * upward).astype(jnp.bfloat16)
    result = jnp.dot(hidden, down_weight_experts[0], preferred_element_type=jnp.float32)
    spread_rows = lax.optimization_barrier(
        result.astype(jnp.bfloat16).reshape(incoming.shape)
    ).astype(jnp.float32)
    summed = lax.psum_scatter(
        spread_rows.astype(jnp.bfloat16), "tp", scatter_dimension=0, tiled=True
    )
    expert_out = lax.all_to_all(summed, "sp", split_axis=0, concat_axis=0, tiled=True)
    table = expert_out.reshape(experts * capacity, expert_out.shape[-1])
    fetched = jnp.take(table, target, axis=0).astype(jnp.float32)
    weighted = jnp.sum(
        fetched.reshape(local_rows, top_count, -1) * routed_expert_weight[:, :, None], axis=1
    )
    return (stream + weighted).astype(jnp.bfloat16)


def solution(mesh):
    return jax.shard_map(
        local,
        mesh=mesh,
        in_specs=(
            P(("grp", "sp"), "tp"),
            P(("grp", "sp"), "tp"),
            P(("grp", "sp"), "tp"),
            P(("grp", "sp"), "tp"),
            P(("grp", "sp"), "tp"),
            P(("grp", "sp"), "tp"),
            P(("grp", "sp"), "tp"),
            P("tp"),
            P("tp"),
            P("tp"),
            P("tp"),
            P("tp", None),
            P(("grp", "sp", "tp"), None),
            P(),
            P(("grp", "sp", "tp"), None),
            P(("grp", "sp", "tp"), None),
            P("sp", None, "tp"),
            P("sp", None, "tp"),
            P("sp", "tp", None),
        ),
        out_specs=P(("grp", "sp", "tp"), None),
        check_vma=False,
    )
```

profile of v0, /device:TPU:0, one launch (start us, length us, event | category | flops | bytes accessed | tf_op | source)
XLA Modules:
  0.0 529.3 jit_solution(16448836899378870690)
XLA Ops:
  6.6 2.0 fusion.60
  8.6 1.8 neg.35
  10.5 2.1 fusion.26
  12.6 2.5 fusion.24
  15.2 1.8 reshape.168
  17.0 1.8 reshape.167
  18.8 3.9 fusion.23
  23.0 1.8 reshape.157
  24.8 6.1 %fusion.20 = (f32[8,8,64,64]{3,2,1,0:T(8,128)S(1)}, f32[8,8,64,64]{3,2,1,0:T(8,128)S(1)}) fusion(f32[8,64,8,64]{3,2,1,0:T(8,128)} %reshape.157, f32[8,8,64,64]{3,1,2,0:T(8,128)} %fusion.24, f32[8,64,8,64]{3,2,1,0:T(8,128)} %reshape.168, f32[8,8,64]{2,1,0:T(8,128)S(1)} %add_rsqrt_fusion, f32[8,64,8]{1,2,0:T(8,128)S(1)} %copy.161, f32[8,64,8,64]{3,2,1,0:T(8,128)} %neg.35), kind=kLoop, calls=%fused_computation.36 | loop fusion | flops 2097152 | bytes 6324224 | tf_op jit(solution)/shard_map/mul | solution.py:108
  31.0 5.4 %fusion.106 = f32[8,8,64,64]{3,2,1,0:T(8,128)} fusion(f32[8,8,64,64]{3,2,1,0:T(8,128)S(1)} %get-tuple-element.199, f32[8,8,64,64]{3,1,2,0:T(8,128)S(1)} %copy-done.1, f32[8,64,8,64]{3,2,1,0:T(8,128)S(1)} %copy-done.4), kind=kOutput, calls=%fused_computation.153 | convolution fusion | flops 201850880 | bytes 4194304 | tf_op jit(solution)/shard_map/bhtn,bhsn->bhts/dot_general | solution.py:34
  36.4 3.4 fusion.109
  39.9 5.3 %fusion.105 = f32[8,8,64,64]{3,2,1,0:T(8,128)} fusion(f32[8,8,64,64]{3,2,1,0:T(8,128)S(1)} %get-tuple-element.198, f32[8,64,8,64]{3,2,1,0:T(8,128)S(1)} %copy-done.6, f32[8,8,64,64]{3,1,2,0:T(8,128)S(1)} %copy-done.1), kind=kOutput, calls=%fused_computation.152 | convolution fusion | flops 201588736 | bytes 4194304 | tf_op jit(solution)/shard_map/bhtn,bhsn->bhts/dot_general | solution.py:34
  45.2 2.4 fusion.42
  47.7 3.6 fusion.110
  51.2 3.8 add_add_fusion.1
  55.1 9.7 %fusion.104 = f32[8,8,64,64]{3,2,1,0:T(8,128)} fusion(f32[8,64,8,64]{3,2,1,0:T(8,128)} %reshape.167, f32[8,8,64,64]{3,1,2,0:T(8,128)} %fusion.24, f32[8,64,8,64]{3,2,1,0:T(8,128)} %reshape.168), kind=kOutput, calls=%fused_computation.151 | convolution fusion | flops 202113024 | bytes 4194304 | tf_op jit(solution)/shard_map/bhtn,bhsn->bhts/dot_general | solution.py:34
  64.9 2.7 fusion.112
  67.6 2.3 fusion.111
  70.0 2.3 fusion.113
  72.2 2.4 convolution_add_fusion.1
  74.7 3.6 fusion.115
  78.2 3.8 fusion.114
  82.1 1.6 reshape.158
  85.2 1.7 copy.187
  87.0 5.5 %convolution_add_fusion = f32[8,8,64,64]{3,2,1,0:T(8,128)S(1)} fusion(f32[8,8,64,64]{3,2,1,0:T(8,128)} %fusion.115, f32[8,8,64,64]{3,2,1,0:T(8,128)} %copy-done.16, f32[8,8,64,64]{3,2,1,0:T(8,128)} %fusion.114), kind=kOutput, calls=%fused_computation.77 | convolution fusion | flops 201850880 | bytes 4194304 | tf_op jit(solution)/shard_map/bhts,bhsu->bhtu/dot_general | solution.py:46
  92.5 2.2 fusion.116
  94.8 1.8 fusion.31
  96.6 3.7 fusion.117
  100.3 2.0 fusion.29
  102.3 5.2 multiply_add_fusion
  107.5 3.6 fusion.47
  111.1 4.9 fusion.45
  116.0 3.6 bitcast_add_fusion.2
  119.6 54.2 %while.30 = (s32[]{:T(128)}, f32[8,64,64]{1,2,0:T(8,128)S(1)}, f32[8,64,64]{1,2,0:T(8,128)}, f32[8,8,64,64]{2,3,1,0:T(8,128)}, f32[8,8,64,64]{2,3,1,0:T(8,128)},...) while((s32[]{:T(128)}, f32[8,64,64]{1,2,0:T(8,128)S(1)}, ...), condition=%wide.region_3.4_spmd.clone, body=%wide.region_2.3_spmd.clone.sunk | while | flops 50429952 | bytes 3016300 | solution.py:134
  122.7 2.3 fusion.170
  125.0 1.5 convolution_bitcast_fusion.4
  129.5 2.3 fusion.170
  136.3 2.3 fusion.170
  143.0 2.3 fusion.170
  149.7 2.3 fusion.170
  156.5 2.3 fusion.170
  163.2 2.3 fusion.170
  165.5 1.5 convolution_bitcast_fusion.4
  170.0 2.3 fusion.170
  173.9 24.6 %all-gather = f32[32,64,64]{2,1,0:T(8,128)} all-gather(f32[8,64,64]{2,1,0:T(8,128)S(1)} %copy.180), channel_id=2, replica_groups=mesh['grp'=2,'sp'=4,'tp'=4] {'sp'}, dimensions={0}, use_global_device_ids=true | all-gather | bytes 655360 | tf_op jit(solution)/shard_map/all_gather | solution.py:16
  199.6 21.8 %all-gather.1 = f32[32,64,64]{2,1,0:T(8,128)} all-gather(f32[8,64,64]{2,1,0:T(8,128)S(1)} %copy.181), channel_id=3, replica_groups=mesh['grp'=2,'sp'=4,'tp'=4] {'sp'}, dimensions={0}, use_global_device_ids=true | all-gather | bytes 655360 | tf_op jit(solution)/shard_map/all_gather | solution.py:16
  221.5 3.7 fusion.87
  225.3 6.7 %fusion.19 = f32[8,8,64,64]{2,3,1,0:T(8,128)S(1)} fusion(f32[8,8,64,64]{2,3,1,0:T(8,128)} %get-tuple-element.93, f32[8,8,64,64]{3,2,0,1:T(8,128)S(1)} %fusion.87, f32[8,8,64,64]{3,2,1,0:T(8,128)} %fusion.47, f32[8,64,8,64]{3,2,1,0:T(8,128)S(1)} %copy-done.7, f32[8,8,64,64]{3,1,2,0:T(8,128)S(1)} %copy-done.3), kind=kOutput, calls=%fused_computation.33 | convolution fusion | flops 202113024 | bytes 6291456 | tf_op jit(solution)/shard_map/bhtk,bhvk->bhtv/dot_general | solution.py:140
  232.0 2.0 fusion.108
  236.0 3.5 fusion.18
  239.5 3.1 copy.189
  242.6 1.9 reshape.160
  244.5 4.3 fusion.83
  251.9 48.6 %reduce-scatter.3.cloned.1.call-done = f32[128,2048]{1,0:T(8,128)} async-done(((f32[512,2048]{1,0:T(8,128)}), f32[128,2048]{1,0:T(8,128)}) %reduce-scatter.3.cloned.1.call-update) | async-done | bytes 1048592 | tf_op jit(solution)/shard_map/reduce_scatter | solution.py:191
  302.7 41.3 %all_to_all.10 = bf16[4,96,2048]{2,1,0:T(8,128)(2,1)} all-to-all(bf16[4,96,2048]{2,1,0:T(8,128)(2,1)S(1)} %bitcast.191), channel_id=1, replica_groups=mesh['grp'=2,'sp'=4,'tp'=4] {'sp'}, dimensions={0} | all-to-all | bytes 3145728 | tf_op jit(solution)/shard_map/all_to_all | solution.py:220
  344.1 44.6 %all-gather.4.cloned.1.call-done = bf16[16,96,2048]{2,1,0:T(8,128)(2,1)} async-done(((bf16[4,96,2048]{2,1,0:T(8,128)(2,1)}), bf16[16,96,2048]{2,1,0:T(8,128)(2,1)}) %all-gather.4.cloned.1.call-update) | async-done | bytes 6291472 | tf_op jit(solution)/shard_map/all_gather | solution.py:219
  388.7 6.0 %fusion.64 = f32[1536,256]{1,0:T(8,128)} fusion(bf16[1536,2048]{1,0:T(8,128)(2,1)} %bitcast.198, bf16[1,2048,256]{2,1,0:T(8,128)(2,1)} %param.39), kind=kOutput, calls=%fused_computation.87 | convolution fusion | flops 1610612736 | bytes 8912896 | tf_op jit(solution)/shard_map/dot_general | solution.py:226
  394.7 12.8 %convolution_convert_fusion = bf16[1536,2048]{1,0:T(8,128)(2,1)} fusion(bf16[1536,2048]{1,0:T(8,128)(2,1)} %bitcast.199, f32[1536,256]{1,0:T(8,128)} %fusion.64, bf16[1,256,2048]{2,1,0:T(8,128)(2,1)} %param.41, bf16[1,2048,256]{2,1,0:T(8,128)(2,1)} %param.40), kind=kOutput, calls=%fused_computation.23 | convolution fusion | flops 3226730496 | bytes 16252928 | tf_op jit(solution)/shard_map/dot_general | solution.py:229
  407.6 59.0 %reduce-scatter.5.cloned.1.call-done = bf16[4,96,2048]{2,1,0:T(8,128)(2,1)} async-done(((bf16[16,96,2048]{2,1,0:T(8,128)(2,1)}), bf16[4,96,2048]{2,1,0:T(8,128)(2,1)}) %reduce-scatter.5.cloned.1.call-update) | async-done | bytes 1572880 | tf_op jit(solution)/shard_map/reduce_scatter | solution.py:233
  466.6 4.9 all-to-all-start.1
  472.0 36.3 %all-to-all-done.1 = bf16[4,96,2048]{2,1,0:T(8,128)(2,1)} async-done(((bf16[4,96,2048]{2,1,0:T(8,128)(2,1)}), bf16[4,96,2048]{2,1,0:T(8,128)(2,1)}, u32[]{:S(2)}, u32[]{:S(2)}) %all-to-all-start.1) | async-done | bytes 1572896 | tf_op jit(solution)/shard_map/all_to_all | solution.py:236
  508.4 5.0 gather_fusion
  513.4 2.5 gather.7
  515.9 5.5 %multiply_reduce_fusion = f32[128,2048]{1,0:T(8,128)S(1)} fusion(bf16[128,2,2048]{2,1,0:T(2,128)(2,1)} %gather.7, pred[128,2]{1,0:T(8,128)(4,1)S(1)} %copy.195, f32[128,2]{1,0:T(8,128)S(1)} %copy.197), kind=kLoop, calls=%fused_computation.49 | loop fusion | flops 1835008 | bytes 2098432 | tf_op jit(solution)/shard_map/reduce_sum | solution.py:239
  (172 shorter events, 44.7 us)
Async XLA Ops:
  6.5 238.0 %copy-start = (bf16[512,2048]{1,0:T(8,128)(2,1)S(1)}, bf16[512,2048]{1,0:T(8,128)(2,1)}, u32[]{:S(2)}) copy-start(bf16[512,2048]{1,0:T(8,128)(2,1)} %param.34) | copy-start | bytes 6291460
  6.5 294.0 %reduce-scatter.3.cloned.1.call-start = ((), (), s32[]{:S(2)}) async-start(), calls=%async_computation.4 | async-start | bytes 5242880 | tf_op jit(solution)/shard_map/reduce_scatter | solution.py:191
  6.6 3.8 copy-start.28
  12.6 2.6 copy-start.25
  15.2 1.8 copy-start.26
  15.2 3.6 copy-start.32
  18.8 3.9 copy-start.27
  18.8 3.9 copy-start.31
  24.8 6.2 %copy-start.1 = (f32[8,8,64,64]{3,1,2,0:T(8,128)S(1)}, f32[8,8,64,64]{3,1,2,0:T(8,128)}, u32[]{:S(2)}) copy-start(f32[8,8,64,64]{3,1,2,0:T(8,128)} %fusion.24) | copy-start | bytes 3145732
  24.8 6.2 %copy-start.4 = (f32[8,64,8,64]{3,2,1,0:T(8,128)S(1)}, f32[8,64,8,64]{3,2,1,0:T(8,128)}, u32[]{:S(2)}) copy-start(f32[8,64,8,64]{3,2,1,0:T(8,128)} %reshape.168) | copy-start | bytes 3145732
  31.0 5.4 %copy-start.11 = (f32[8,8,64,64]{3,2,1,0:T(8,128)}, f32[8,8,64,64]{3,2,1,0:T(8,128)S(1)}, u32[]{:S(2)}) copy-start(f32[8,8,64,64]{3,2,1,0:T(8,128)S(1)} %get-tuple-element.199) | copy-start | bytes 3145732
  31.0 8.9 %copy-start.8 = (f32[8,8,64,64]{3,2,1,0:T(8,128)}, f32[8,8,64,64]{3,2,1,0:T(8,128)S(1)}, u32[]{:S(2)}) copy-start(f32[8,8,64,64]{3,2,1,0:T(8,128)S(1)} %get-tuple-element.198) | copy-start | bytes 3145732
  36.4 3.5 copy-start.6
  55.1 9.8 %copy-start.10 = (f32[8,8,64,64]{3,2,1,0:T(8,128)S(1)}, f32[8,8,64,64]{3,2,1,0:T(8,128)}, u32[]{:S(2)}) copy-start(f32[8,8,64,64]{3,2,1,0:T(8,128)} %fusion.110) | copy-start | bytes 3145732
  64.9 2.7 copy-start.13
  74.6 3.6 copy-start.16
  83.7 1.5 copy-start.19
  87.0 13.3 %copy-start.17 = (bf16[8,8,64,64]{2,3,1,0:T(8,128)(2,1)}, bf16[8,8,64,64]{2,3,1,0:T(8,128)(2,1)S(1)}, u32[]{:S(2)}) copy-start(bf16[8,8,64,64]{2,3,1,0:T(8,128)(2,1)S(1)} %copy.187) | copy-start | bytes 1572868
  87.0 5.5 %copy-start.12 = (f32[8,8,64,64]{3,2,1,0:T(8,128)S(1)}, f32[8,8,64,64]{3,2,1,0:T(8,128)}, u32[]{:S(2)}) copy-start(f32[8,8,64,64]{3,2,1,0:T(8,128)} %copy-done.11) | copy-start | bytes 3145732
  92.5 2.2 copy-start.21
  96.5 3.8 copy-start.2
  96.6 3.8 copy-start.5
  100.3 2.0 copy-start.9
  102.3 5.2 copy-start.14
  221.5 3.7 copy-start.3
  221.5 3.7 copy-start.7
  225.2 6.7 %copy-start.18 = (bf16[8,8,64,64]{2,3,1,0:T(8,128)(2,1)S(1)}, bf16[8,8,64,64]{2,3,1,0:T(8,128)(2,1)}, u32[]{:S(2)}) copy-start(bf16[8,8,64,64]{2,3,1,0:T(8,128)(2,1)} %copy-done.17) | copy-start | bytes 1572868
  225.2 6.7 %copy-start.20 = (f32[8,8,64,64]{3,2,1,0:T(8,128)S(1)}, f32[8,8,64,64]{3,2,1,0:T(8,128)}, u32[]{:S(2)}) copy-start(f32[8,8,64,64]{3,2,1,0:T(8,128)} %fusion.104) | copy-start | bytes 3145732
  225.2 6.7 %copy-start.22 = (f32[8,8,64,64]{2,3,1,0:T(8,128)S(1)}, f32[8,8,64,64]{2,3,1,0:T(8,128)}, u32[]{:S(2)}) copy-start(f32[8,8,64,64]{2,3,1,0:T(8,128)} %fusion.45) | copy-start | bytes 3145732
  234.0 1.3 copy-start.15
  234.0 1.8 copy-start.33
  234.0 2.0 copy-start.24
  248.8 0.7 copy-start.29
  248.8 53.0 %copy-start.23 = (bf16[128,2048]{1,0:T(8,128)(2,1)S(1)}, bf16[128,2048]{1,0:T(8,128)(2,1)}, u32[]{:S(2)}) copy-start(bf16[128,2048]{1,0:T(8,128)(2,1)} %param.35) | copy-start | bytes 1572868
  248.8 53.2 %copy-start.30 = (f32[2048]{0:T(1024)S(1)}, f32[2048]{0:T(1024)}, u32[]{:S(2)}) copy-start(f32[2048]{0:T(1024)} %param.36) | copy-start | bytes 24580
  248.9 139.9 %all-gather.4.cloned.1.call-start = ((), (), s32[]{:S(2)}) async-start(), calls=%async_computation.5 | async-start | bytes 7864320 | tf_op jit(solution)/shard_map/all_gather | solution.py:219
  344.1 122.5 %reduce-scatter.5.cloned.1.call-start = ((), (), s32[]{:S(2)}) async-start(), calls=%async_computation.6 | async-start | bytes 7864320 | tf_op jit(solution)/shard_map/reduce_scatter | solution.py:233
  407.6 64.3 %copy-start.34 = (f32[128,2]{0,1:T(2,128)S(1)}, f32[128,2]{0,1:T(2,128)}, u32[]{:S(2)}) copy-start(f32[128,2]{0,1:T(2,128)} %param.38) | copy-start | bytes 3076
  466.6 41.8 %all-to-all-start.1 = ((bf16[4,96,2048]{2,1,0:T(8,128)(2,1)}), bf16[4,96,2048]{2,1,0:T(8,128)(2,1)}, u32[]{:S(2)}, u32[]{:S(2)}) async-start(bf16[4,96,2048]{2,1,0:T(8,128)(2,1)} %reduce-scatter.5.cloned.1.call-done), calls=%async_computation.3 | async-start | bytes 3145728 | tf_op jit(solution)/shard_map/all_to_all | solution.py:236
Sparse Core Ops, SparseCore 0:
  249.0 51.5 reduce-scatter.2
  344.2 44.4 all-gather.3
  407.7 58.8 reduce-scatter.4
where the time goes:
time: 537 us; the launch traced here: 529 us
  waiting for transfers between devices  189 us (35%)
  matrix products  150 us (28%)
  blocking collectives  87.8 us (16%)
  local copies, waits for them, and re-layouts  46.1 us (9%)
  other arithmetic  37.4 us (7%)
  between operations  14.3 us (3%)
    reduce_scatter x1, waiting for transfers between devices, local(): lax.psum_scatter(spread_rows.astype(jnp.bfloat16), 'tp', scatter_dimensio...  59 us
    reduce_scatter x1, waiting for transfers between devices, local(): lax.psum_scatter(jnp.dot(attention_result, output_weight_matrix, preferre...  48.6 us
    all_gather x2, blocking collectives, prefix_2(): gathered = jax.tree.map(lambda a: lax.all_gather(a, axis), part)  46.5 us
    all_gather x1, waiting for transfers between devices, local(): lax.all_gather(lax.all_to_all(outgoing, 'sp', split_axis=0, concat_axis=0...  44.6 us
    all_to_all x1, blocking collectives, local(): lax.all_to_all(outgoing, 'sp', split_axis=0, concat_axis=0, tiled=True)  41.3 us
    all_to_all x1, waiting for transfers between devices, local(): lax.all_to_all(summed, 'sp', split_axis=0, concat_axis=0, tiled=True)  36.3 us
    dot_general x10, matrix products, square_blocks(): return jnp.einsum('bhts,bhsu->bhtu', left, right, precision=PRECISE)  32.5 us
    dot_general x4, matrix products, pair_scores(): return jnp.einsum('bhtn,bhsn->bhts', left, right, precision=PRECISE)  23.9 us
  transfers between devices with their start and end apart: 4, of which 4 were waited for; matrix products, arithmetic and copies ran while one was open for 1% of the time, Pallas kernels for 0%

commit v1 on v0

v1 whole, which is shorter than its diff:
```python
import functools

import jax
import jax.numpy as jnp
from jax import lax
from jax.experimental import pallas as pl
from jax.experimental.pallas import tpu as pltpu
from jax.sharding import PartitionSpec as P

SPAN = 64
SUB = 16
LANES = 256
GROUP_EPS = 0.00064
NORM_EPS = 1e-06
NN = (((1,), (0,)), ((), ()))
NT = (((1,), (1,)), ((), ()))
TN = (((0,), (0,)), ((), ()))


def halves(x):
    high = x.astype(jnp.bfloat16)
    return high, (x - high.astype(jnp.float32)).astype(jnp.bfloat16)


def product(left, right, dims):
    def dot(a, b):
        return lax.dot_general(a, b, dims, preferred_element_type=jnp.float32)

    return dot(left[0], right[0]) + (dot(left[1], right[0]) + dot(left[0], right[1]))


def block_mask(head_width):
    rows = lax.broadcasted_iota(jnp.int32, (LANES, LANES), 0) // head_width
    lanes = lax.broadcasted_iota(jnp.int32, (LANES, LANES), 1) // head_width
    return jnp.where(rows == lanes, 1.0, 0.0)


def spread_blocks(x, mask):
    copies = LANES // x.shape[0]
    return tuple(jnp.concatenate([part] * copies, axis=0) * mask for part in halves(x))


def head_sum(x, mask):
    high, low = halves(x)
    return lax.dot_general(
        high, mask, NN, preferred_element_type=jnp.float32
    ) + lax.dot_general(low, mask, NN, preferred_element_type=jnp.float32)


def chunk_kernel(
    head_width,
    recept_ref,
    key_ref,
    value_ref,
    decay_ref,
    rate_ref,
    offset_ref,
    decay_bias_ref,
    rate_bias_ref,
    map_ref,
    own_ref,
    transit_ref,
    added_ref,
):
    span = head_width
    wide_mask = block_mask(head_width)
    mask = wide_mask.astype(jnp.bfloat16)
    per_group = LANES // head_width
    times = lax.broadcasted_iota(jnp.int32, (span, LANES), 0)
    lanes = lax.broadcasted_iota(jnp.int32, (span, LANES), 1)
    earlier = lanes % head_width
    strict = times > earlier
    within = times >= earlier
    eye = jnp.where(times == earlier, 1.0, 0.0)
    same = (times // SUB) == (earlier // SUB)
    tri = jnp.where(
        lax.broadcasted_iota(jnp.int32, (span, span), 0)
        >= lax.broadcasted_iota(jnp.int32, (span, span), 1),
        1.0,
        0.0,
    ).astype(jnp.bfloat16)

    @pl.when(pl.program_id(0) == 0)
    def _():
        full_lanes = lax.broadcasted_iota(jnp.int32, transit_ref.shape, 1) % head_width
        full_rows = lax.broadcasted_iota(jnp.int32, transit_ref.shape, 0)
        transit_ref[...] = jnp.where(full_lanes == full_rows, 1.0, 0.0)
        added_ref[...] = jnp.zeros_like(added_ref)

    spread = functools.partial(spread_blocks, mask=mask)
    row_count, channel_width = recept_ref.shape
    cells = [
        (group, chunk)
        for chunk in range(row_count // span)
        for group in range(channel_width // LANES)
    ]

    def prepare(group, chunk):
        at = (slice(chunk * span, (chunk + 1) * span), slice(group * LANES, (group + 1) * LANES))
        cols = at[1]
        recept = recept_ref[at].astype(jnp.float32)
        key = key_ref[at].astype(jnp.float32)
        value = value_ref[at].astype(jnp.float32)
        offset = jnp.zeros((span, LANES), jnp.float32)
        for head in range(per_group):
            column = group * per_group + head
            offset = jnp.where(
                lanes // head_width == head, offset_ref[at[0], column : column + 1], offset
            )
        pre = decay_bias_ref[:, cols] + decay_ref[at].astype(jnp.float32)
        decay = offset - 0.6065306597126334 / (1.0 + jnp.exp(-pre))
        rate = 1.0 / (
            1.0 + jnp.exp(-(rate_bias_ref[:, cols] + rate_ref[at].astype(jnp.float32)))
        )
        unit = key * lax.rsqrt(head_sum(key * key, mask) + NORM_EPS)
        one, rest = halves(decay)
        third = (decay - one.astype(jnp.float32) - rest.astype(jnp.float32)).astype(jnp.bfloat16)
        cumul = sum(
            lax.dot_general(tri, part, NN, preferred_element_type=jnp.float32)
            for part in (third, rest, one)
        )
        middle = cumul[span // 2 : span // 2 + 1]
        last = cumul[span - 1 : span]
        center = cumul - middle
        shrink = jnp.exp(center)
        grow = jnp.exp(-center)
        remove = -unit * jnp.exp(center - decay)
        reads = recept * shrink
        write = unit * rate * grow
        keys = key * grow
        left = halves(jnp.concatenate([remove, reads], axis=0))
        by_write = product(left, spread(write), NT)
        by_key = product(left, spread(keys), NT)
        remove_write = jnp.where(strict, by_write[:span], 0.0)
        read_write = halves(jnp.where(within, by_write[span:], 0.0))
        key_rows = halves(
            jnp.concatenate(
                [jnp.where(strict, by_key[:span], 0.0), jnp.where(within, by_key[span:], 0.0)],
                axis=0,
            )
        )
        power = jnp.where(same, remove_write, 0.0)
        inverse = eye + power
        power = product(halves(power), spread(power), NN)
        reach = 2
        while reach < SUB:
            factor = spread(power)
            if reach * 2 < SUB:
                both = product(
                    halves(jnp.concatenate([inverse, power], axis=0)), factor, NN
                )
                inverse = inverse + both[:span]
                power = both[span:]
            else:
                inverse = inverse + product(halves(inverse), factor, NN)
            reach *= 2
        size = SUB
        while size < span:
            joint = (times // (2 * size) == earlier // (2 * size)) & (
                times // size != earlier // size
            )
            step = product(
                halves(inverse), spread(jnp.where(joint, remove_write, 0.0)), NN
            )
            inverse = inverse + product(halves(step), spread(inverse), NN)
            size *= 2
        inverse = halves(inverse)
        start = jnp.exp(middle)
        from_value = product(key_rows, spread(value), NN)
        inv_remove = product(inverse, spread(remove), NN) * start
        inv_value = product(inverse, spread(from_value[:span]), NN)
        read_map = reads * start + product(read_write, spread(inv_remove), NN)
        read_own = from_value[span:] + product(read_write, spread(inv_value), NN)
        tail = jnp.exp(last - middle)
        write_end = write * tail
        key_end = keys * tail
        transit = product(halves(inv_remove.T), halves(write_end), NN)
        transit = transit * wide_mask
        full = jnp.concatenate([jnp.exp(last)] * (LANES // 8), axis=0)
        full = jnp.concatenate([full] * 8, axis=0)
        diagonal = lax.broadcasted_iota(jnp.int32, (LANES, LANES), 0) == (
            lax.broadcasted_iota(jnp.int32, (LANES, LANES), 1)
        )
        transit = transit + jnp.where(diagonal, full, 0.0)
        added = product(
            halves(jnp.concatenate([inv_value, value], axis=0).T),
            halves(jnp.concatenate([write_end, key_end], axis=0)),
            NN,
        )
        added = added * wide_mask
        added = sum(added[h * head_width : (h + 1) * head_width] for h in range(per_group))
        return at, read_map, read_own, transit, added

    for group, chunk in cells:
        at, read_map, read_own, transit, added = prepare(group, chunk)
        cols = at[1]
        held_transit = transit_ref[:, cols]
        held_added = added_ref[:, cols]
        rows = halves(read_map)
        map_ref[at] = product(rows, spread(held_transit), NT)
        own_ref[at] = read_own + product(rows, spread(held_added), NT)
        moved = product(
            halves(jnp.concatenate([held_transit, held_added], axis=0)), halves(transit), NN
        )
        transit_ref[:, cols] = moved[:span]
        added_ref[:, cols] = moved[span:] + added


def advance_kernel(head_width, state_ref, transit_ref, added_ref, out_ref):
    mask = block_mask(head_width).astype(jnp.bfloat16)
    for group in range(state_ref.shape[1] // LANES):
        cols = slice(group * LANES, (group + 1) * LANES)
        out_ref[:, cols] = added_ref[:, cols] + product(
            halves(state_ref[:, cols]), spread_blocks(transit_ref[:, cols], mask), NN
        )


def finish_kernel(
    head_width,
    map_ref,
    own_ref,
    state_ref,
    recept_ref,
    key_ref,
    value_ref,
    gate_ref,
    gain_ref,
    self_ref,
    out_ref,
):
    mask = block_mask(head_width).astype(jnp.bfloat16)
    for group in range(map_ref.shape[1] // LANES):
        cols = slice(group * LANES, (group + 1) * LANES)
        read = own_ref[:, cols] + product(
            halves(map_ref[:, cols]), spread_blocks(state_ref[:, cols], mask), NT
        )
        off = read - head_sum(read, mask) * (1.0 / head_width)
        spread = head_sum(off * off, mask) * (1.0 / head_width)
        normed = off * lax.rsqrt(spread + GROUP_EPS) * gain_ref[:, cols]
        own = head_sum(
            recept_ref[:, cols].astype(jnp.float32)
            * key_ref[:, cols].astype(jnp.float32)
            * self_ref[:, cols],
            mask,
        ) * value_ref[:, cols].astype(jnp.float32)
        out_ref[:, cols] = ((normed + own) * gate_ref[:, cols].astype(jnp.float32)).astype(
            jnp.bfloat16
        )


def mixer(
    recept,
    key_input,
    value_input,
    output_gate_input,
    decay_input_part,
    correction_rate_input,
    head_decay_offset,
    decay_fixed_bias,
    correction_rate_bias,
    head_norm_gain,
    self_term_weight,
    axis_size,
):
    length, width = recept.shape
    heads = head_decay_offset.shape[1]
    head_width = width // heads
    rows = 2 * SPAN
    by_rows = pl.BlockSpec((rows, width), lambda i: (i, 0))
    fixed = pl.BlockSpec((1, width), lambda i: (0, 0))
    states = pl.BlockSpec((head_width, width), lambda i: (0, 0))
    wide = jax.ShapeDtypeStruct((length, width), jnp.float32)
    small = jax.ShapeDtypeStruct((head_width, width), jnp.float32)
    params = pltpu.CompilerParams(dimension_semantics=("arbitrary",))
    read_map, read_own, transit, added = pl.pallas_call(
        functools.partial(chunk_kernel, head_width),
        grid=(length // rows,),
        in_specs=[by_rows] * 5
        + [pl.BlockSpec((rows, heads), lambda i: (i, 0)), fixed, fixed],
        out_specs=[by_rows, by_rows, states, states],
        out_shape=[wide, wide, small, small],
        compiler_params=params,
        cost_estimate=pl.CostEstimate(
            flops=30_000_000_000, bytes_accessed=8 * length * width, transcendentals=0
        ),
        name="chunks",
    )(
        recept,
        key_input,
        value_input,
        decay_input_part,
        correction_rate_input,
        head_decay_offset,
        decay_fixed_bias[None],
        correction_rate_bias[None],
    )
    place = lax.axis_index("sp")
    state = jnp.zeros_like(added)
    for lap in range(axis_size - 1):
        sent = added
        if lap > 0:
            sent = pl.pallas_call(
                functools.partial(advance_kernel, head_width), out_shape=small, name="advance"
            )(state, transit, added)
        got = lax.ppermute(sent, "sp", [(i, i + 1) for i in range(axis_size - 1)])
        state = jnp.where(place == lap + 1, got, state)
    return pl.pallas_call(
        functools.partial(finish_kernel, head_width),
        grid=(length // rows,),
        in_specs=[by_rows, by_rows, states] + [by_rows] * 4 + [fixed, fixed],
        out_specs=by_rows,
        out_shape=jax.ShapeDtypeStruct((length, width), jnp.bfloat16),
        compiler_params=params,
        name="finish",
    )(
        read_map,
        read_own,
        state,
        recept,
        key_input,
        value_input,
        output_gate_input,
        head_norm_gain[None],
        self_term_weight[None],
    )


def local(
    recept,
    key_input,
    value_input,
    output_gate_input,
    decay_input_part,
    correction_rate_input,
    head_decay_offset,
    decay_fixed_bias,
    correction_rate_bias,
    head_norm_gain,
    self_term_weight,
    output_weight_matrix,
    residual,
    feedforward_norm_gain,
    routed_expert_index,
    routed_expert_weight,
    gate_weight_experts,
    up_weight_experts,
    down_weight_experts,
):
    gates = lax.all_gather(gate_weight_experts, "tp", axis=0)
    ups = lax.all_gather(up_weight_experts, "tp", axis=0)
    downs = lax.all_gather(down_weight_experts, "tp", axis=0)
    attention_result = mixer(
        recept,
        key_input,
        value_input,
        output_gate_input,
        decay_input_part,
        correction_rate_input,
        head_decay_offset,
        decay_fixed_bias,
        correction_rate_bias,
        head_norm_gain,
        self_term_weight,
        lax.axis_size("sp"),
    )
    proj = lax.psum_scatter(
        jnp.dot(
            attention_result, output_weight_matrix, preferred_element_type=jnp.float32
        ).astype(jnp.bfloat16),
        "tp",
        scatter_dimension=0,
        tiled=True,
    )
    stream = residual.astype(jnp.float32) + lax.optimization_barrier(proj).astype(jnp.float32)
    ffn_in = (
        stream
        * lax.rsqrt(jnp.mean(stream * stream, axis=-1, keepdims=True) + NORM_EPS)
        * feedforward_norm_gain
    ).astype(jnp.bfloat16)
    width = ffn_in.shape[1]
    local_experts = gate_weight_experts.shape[0]
    experts = local_experts * lax.axis_size("sp")
    ids = jnp.arange(experts, dtype=jnp.int32)
    shares = jnp.sum(
        jnp.where(
            routed_expert_index[:, :, None] == ids, routed_expert_weight[:, :, None], 0.0
        ),
        axis=1,
    )
    first = shares.astype(jnp.bfloat16)
    rest = shares - first.astype(jnp.float32)
    second = rest.astype(jnp.bfloat16)
    third = (rest - second.astype(jnp.float32)).astype(jnp.bfloat16)
    extra = jnp.concatenate([first, second, third], axis=1)
    extra = jnp.pad(extra, ((0, 0), (0, -extra.shape[1] % 128)))
    packed = lax.all_gather(
        jnp.concatenate([ffn_in, extra], axis=1), "sp", axis=0, tiled=True
    )
    features = packed[:, :width]
    tail = packed[:, width : width + 3 * experts].astype(jnp.float32)
    shares = tail[:, :experts] + tail[:, experts : 2 * experts] + tail[:, 2 * experts :]
    total = None
    for own in range(local_experts):
        expert = lax.axis_index("sp") * local_experts + own
        share = jnp.sum(jnp.where(ids[None, :] == expert, shares, 0.0), axis=1, keepdims=True)
        gated = jnp.einsum(
            "rd,jdf->jrf", features, gates[:, own], preferred_element_type=jnp.float32
        )
        upward = jnp.einsum(
            "rd,jdf->jrf", features, ups[:, own], preferred_element_type=jnp.float32
        )
        hidden = (jax.nn.silu(gated) * upward).astype(jnp.bfloat16)
        result = jnp.einsum(
            "jrf,jfd->rd", hidden, downs[:, own], preferred_element_type=jnp.float32
        )
        term = result * share
        total = term if total is None else total + term
    weighted = lax.psum_scatter(
        total.astype(jnp.bfloat16), "sp", scatter_dimension=0, tiled=True
    )
    return (stream + weighted.astype(jnp.float32)).astype(jnp.bfloat16)


def solution(mesh):
    return jax.shard_map(
        local,
        mesh=mesh,
        in_specs=(
            P(("grp", "sp"), "tp"),
            P(("grp", "sp"), "tp"),
            P(("grp", "sp"), "tp"),
            P(("grp", "sp"), "tp"),
            P(("grp", "sp"), "tp"),
            P(("grp", "sp"), "tp"),
            P(("grp", "sp"), "tp"),
            P("tp"),
            P("tp"),
            P("tp"),
            P("tp"),
            P("tp", None),
            P(("grp", "sp", "tp"), None),
            P(),
            P(("grp", "sp", "tp"), None),
            P(("grp", "sp", "tp"), None),
            P("sp", None, "tp"),
            P("sp", None, "tp"),
            P("sp", "tp", None),
        ),
        out_specs=P(("grp", "sp", "tp"), None),
        check_vma=False,
    )
```

time: 537 us -> 357 us (0.66); the launches traced: 529 us -> 356 us
  matrix products: 150 us -> 20.7 us
  blocking collectives: 87.8 us -> 0 us
  Pallas kernels: 0 us -> 65.1 us
  local copies, waits for them, and re-layouts: 46.1 us -> 2.46 us
  waiting for transfers between devices: 189 us -> 231 us
  other arithmetic: 37.4 us -> 9.65 us
  starting transfers between devices: 4.97 us -> 13.9 us
    dot_general x44 -> x2, matrix products: 146 us -> 17 us  [the longest x1 10.6 us: local(): jnp.einsum('jrf,jfd->rd', hidden, downs[:, own], preferred_element_type=j...]
    all_gather x1 -> x4, waiting for transfers between devices: 44.6 us -> 145 us  [the longest x1 45.8 us: local(): lax.all_gather(jnp.concatenate([ffn_in, extra], axis=1), 'sp', axis=0, ti...]
    pallas_call x0 -> x4, Pallas kernels: none -> 65.1 us  [the longest x1 54.6 us: mixer(): pl.pallas_call(functools.partial(chunk_kernel, head_width), grid=(length...]
    all_gather x2 -> x0, blocking collectives: 46.5 us -> none  [prefix_2(): gathered = jax.tree.map(lambda a: lax.all_gather(a, axis), part)]
    all_to_all x1 -> x0, blocking collectives: 41.3 us -> none  [local(): lax.all_to_all(outgoing, 'sp', split_axis=0, concat_axis=0, tiled=True)]
    all_to_all x1 -> x0, waiting for transfers between devices: 36.3 us -> none  [local(): lax.all_to_all(summed, 'sp', split_axis=0, concat_axis=0, tiled=True)]
    reduce_scatter x1, waiting for transfers between devices: 48.6 us -> 31.6 us  [local(): lax.psum_scatter(jnp.dot(attention_result, output_weight_matrix, preferre...]
    reduce_scatter x1, waiting for transfers between devices: 59 us -> 43.8 us  [local(): lax.psum_scatter(total.astype(jnp.bfloat16), 'sp', scatter_dimension=0, t...]
  transfers between devices with their start and end apart: 4 -> 9, of which waited for: 4 -> 9; matrix products, arithmetic and copies ran while one was open for 1% -> 2% of each run, Pallas kernels for 0% -> 0%
where the time goes in v1:
time: 357 us; the launch traced here: 356 us
  waiting for transfers between devices  231 us (65%)
  Pallas kernels  65.1 us (18%)
  matrix products  20.7 us (6%)
  starting transfers between devices  13.9 us (4%)
  between operations  13.6 us (4%)
  other arithmetic  9.65 us (3%)
    pallas_call x1, Pallas kernels, mixer(): pl.pallas_call(functools.partial(chunk_kernel, head_width), grid=(length...  54.6 us
    all_gather x1, waiting for transfers between devices, local(): lax.all_gather(jnp.concatenate([ffn_in, extra], axis=1), 'sp', axis=0, ti...  45.8 us
    reduce_scatter x1, waiting for transfers between devices, local(): lax.psum_scatter(total.astype(jnp.bfloat16), 'sp', scatter_dimension=0, t...  43.8 us
    all_gather x1, waiting for transfers between devices, local(): downs = lax.all_gather(down_weight_experts, 'tp', axis=0)  35.9 us
    all_gather x1, waiting for transfers between devices, local(): gates = lax.all_gather(gate_weight_experts, 'tp', axis=0)  33.6 us
    reduce_scatter x1, waiting for transfers between devices, local(): lax.psum_scatter(jnp.dot(attention_result, output_weight_matrix, preferre...  31.6 us
    all_gather x1, waiting for transfers between devices, local(): ups = lax.all_gather(up_weight_experts, 'tp', axis=0)  29.4 us
    ppermute x3, starting transfers between devices, mixer(): got = lax.ppermute(sent, 'sp', [(i, i + 1) for i in range(axis_size - 1)])  13.5 us
  transfers between devices with their start and end apart: 9, of which 9 were waited for; matrix products, arithmetic and copies ran while one was open for 2% of the time, Pallas kernels for 0%

profile of v1, /device:TPU:0, one launch (start us, length us, event | category | flops | bytes accessed | tf_op | source)
XLA Modules:
  0.0 355.9 jit_solution(2226987862600532492)
XLA Ops:
  6.5 0.0 copy-start
  6.5 0.0 reduce-scatter.3.cloned.1.call-start
  6.5 1.7 copy.27.offset_ref
  8.2 54.6 %chunks.1 = (f32[512,512]{1,0:T(8,128)}, f32[512,512]{1,0:T(8,128)}, f32[64,512]{1,0:T(8,128)}, f32[64,512]{1,0:T(8,128)}) custom-call(bf16[512,512]{1,0:T(8,128)(2,1)} %recept_ref.3, bf16[512,512]{1,0:T(8,128)(2,1)} %key_ref.3, bf16[512,512]{1,0:T(8,128)(2,1)} %value_ref.3, bf16[512,512]{1,0:T(8,128)(2,1)} %decay_ref.1, bf16[512,512]{1,0:T(8,128)(2,1)} %rate_ref.1, ...), custom_call_target="tpu_custom_call" | custom-call | flops 30000001024 | bytes 2097152 | tf_op jit(solution)/shard_map/chunks/pallas_call | solution.py:275
  62.8 5.0 %collective-permute-start = (f32[64,512]{1,0:T(8,128)}, f32[64,512]{1,0:T(8,128)S(1)}, u32[]{:S(2)}, u32[]{:S(2)}) collective-permute-start(f32[64,512]{1,0:T(8,128)} %get-tuple-element.11.added_ref), channel_id=1, source_target_pairs={{0,4},{4,8},{8,12},{1,5},{5,9},{9,13},{2,6},{6,10},{10,14},{3,7},{... | collective-permute-start | bytes 393224 | tf_op jit(solution)/shard_map/ppermute | solution.py:305
  67.8 3.0 collective-permute-done
  70.9 0.7 broadcast_select_fusion.state_ref
  71.5 2.0 advance.2
  73.5 4.3 %collective-permute-start.1 = (f32[64,512]{1,0:T(8,128)}, f32[64,512]{1,0:T(8,128)S(1)}, u32[]{:S(2)}, u32[]{:S(2)}) collective-permute-start(f32[64,512]{1,0:T(8,128)} %advance.2), channel_id=1, source_target_pairs={{0,4},{4,8},{8,12},{1,5},{5,9},{9,13},{2,6},{6,10},{10,14},{3,7},{... | collective-permute-start | bytes 393224 | tf_op jit(solution)/shard_map/ppermute | solution.py:305
  77.8 2.8 collective-permute-done.1
  80.6 0.7 broadcast_select_fusion.1.state_ref
  81.3 2.0 advance.3
  83.2 4.2 %collective-permute-start.2 = (f32[64,512]{1,0:T(8,128)}, f32[64,512]{1,0:T(8,128)S(1)}, u32[]{:S(2)}, u32[]{:S(2)}) collective-permute-start(f32[64,512]{1,0:T(8,128)} %advance.3), channel_id=1, source_target_pairs={{0,4},{4,8},{8,12},{1,5},{5,9},{9,13},{2,6},{6,10},{10,14},{3,7},{... | collective-permute-start | bytes 393224 | tf_op jit(solution)/shard_map/ppermute | solution.py:305
  87.5 2.8 collective-permute-done.2
  90.3 1.6 broadcast_select_fusion.2.state_ref
  91.8 6.6 %finish.1 = bf16[512,512]{1,0:T(8,128)(2,1)} custom-call(f32[512,512]{1,0:T(8,128)} %get-tuple-element.9.map_ref, f32[512,512]{1,0:T(8,128)} %get-tuple-element.10.own_ref, f32[64,512]{1,0:T(8,128)} %broadcast_select_fusion.2.state_ref, bf16[512,512]{1,0:T(8,128)(2,1)} %recept_ref.3, bf16[512,512]{1,0:T(8,128)(2,1)} %key_ref.3, bf16[512,512]{1,0:T(8,128)(2,1)} %value_ref.3, ...), custom_call_target="tpu_custom_call" | custom-call | tf_op jit(solution)/shard_map/finish/pallas_call | solution.py:307
  98.4 0.0 copy-done
  98.4 3.6 %convolution_convert_fusion = bf16[512,2048]{1,0:T(8,128)(2,1)} fusion(bf16[512,512]{1,0:T(8,128)(2,1)} %finish.1, bf16[512,2048]{1,0:T(8,128)(2,1)S(1)} %copy-done), kind=kOutput, calls=%fused_computation.2 | convolution fusion | flops 1074790400 | bytes 4718592 | tf_op jit(solution)/shard_map/dot_general | solution.py:367
  102.1 0.0 copy-start.4
  102.1 0.0 copy-start.5
  102.1 0.0 copy-start.1
  102.1 0.0 copy-start.3
  102.1 0.0 reduce-scatter.3.cloned.1.call-update
  102.1 0.0 all-gather.8.cloned.1.call-start
  102.2 0.6 copy-done.4
  102.8 0.0 copy-done.5
  102.8 0.1 copy.28
  102.9 31.6 %reduce-scatter.3.cloned.1.call-done = bf16[128,2048]{1,0:T(8,128)(2,1)} async-done(((bf16[512,2048]{1,0:T(8,128)(2,1)}), bf16[128,2048]{1,0:T(8,128)(2,1)}) %reduce-scatter.3.cloned.1.call-update) | async-done | bytes 524304 | tf_op jit(solution)/shard_map/reduce_scatter | solution.py:366
  134.5 0.0 copy-done.1
  134.5 1.3 multiply_reduce_fusion
  135.9 0.0 copy-done.3
  135.9 1.3 multiply_convert_fusion
  137.1 0.8 fusion.7
  138.0 0.0 all-gather.8.cloned.1.call-update
  138.0 0.0 all-gather.10.cloned.1.call-start
  138.0 0.7 all-gather.10.cloned.1.call-update
  138.7 0.0 all-gather.12.cloned.1.call-start
  138.8 0.5 all-gather.12.cloned.1.call-update
  139.3 0.0 all-gather.14.cloned.1.call-start
  139.4 0.5 all-gather.14.cloned.1.call-update
  139.9 0.2 reduce-scatter.5.cloned.1.call-start
  140.1 45.8 %all-gather.8.cloned.1.call-done = bf16[512,2176]{1,0:T(8,128)(2,1)} async-done(((bf16[128,2176]{1,0:T(8,128)(2,1)}), bf16[512,2176]{1,0:T(8,128)(2,1)}) %all-gather.8.cloned.1.call-update) | async-done | bytes 2228240 | tf_op jit(solution)/shard_map/all_gather | solution.py:396
  186.0 0.9 slice_convert_fusion
  186.9 0.3 fusion.9
  187.2 33.6 %all-gather.10.cloned.1.call-done = bf16[4,2048,256]{2,1,0:T(8,128)(2,1)} async-done(((bf16[1,2048,256]{2,1,0:T(8,128)(2,1)}), bf16[4,2048,256]{2,1,0:T(8,128)(2,1)}) %all-gather.10.cloned.1.call-update) | async-done | bytes 4194320 | tf_op jit(solution)/shard_map/all_gather | solution.py:349
  220.8 6.5 %fusion.5 = f32[512,4,256]{2,0,1:T(8,128)} fusion(bf16[4,2048,256]{2,1,0:T(8,128)(2,1)} %all-gather.10.cloned.1.call-done, bf16[512,2176]{1,0:T(8,128)(2,1)} %all-gather.8.cloned.1.call-done), kind=kOutput, calls=%fused_computation.11 | convolution fusion | flops 2147483648 | bytes 8388608 | tf_op jit(solution)/shard_map/rd,jdf->jrf/dot_general | solution.py:406
  227.3 29.4 %all-gather.12.cloned.1.call-done = bf16[4,2048,256]{2,1,0:T(8,128)(2,1)} async-done(((bf16[1,2048,256]{2,1,0:T(8,128)(2,1)}), bf16[4,2048,256]{2,1,0:T(8,128)(2,1)}) %all-gather.12.cloned.1.call-update) | async-done | bytes 4194320 | tf_op jit(solution)/shard_map/all_gather | solution.py:350
  256.7 35.9 %all-gather.14.cloned.1.call-done = bf16[4,256,2048]{2,1,0:T(8,128)(2,1)} async-done(((bf16[1,256,2048]{2,1,0:T(8,128)(2,1)}), bf16[4,256,2048]{2,1,0:T(8,128)(2,1)}) %all-gather.14.cloned.1.call-update) | async-done | bytes 4194320 | tf_op jit(solution)/shard_map/all_gather | solution.py:351
  292.6 10.6 %fusion = bf16[512,2048]{1,0:T(8,128)(2,1)} fusion(bf16[4,256,2048]{2,1,0:T(8,128)(2,1)} %all-gather.14.cloned.1.call-done, f32[512]{0:T(512)S(1)} %fusion.9, f32[512,4,256]{2,0,1:T(8,128)} %fusion.5, bf16[4,2048,256]{2,1,0:T(8,128)(2,1)} %all-gather.12.cloned.1.call-done, bf16[512,2176]{1,0:T(8,128)(2,1)} %all-gather.8.cloned.1.call-done), kind=kOutput, calls=%fused_computation.1 | convolution fusion | flops 4300210176 | bytes 14682112 | tf_op jit(solution)/shard_map/jrf,jfd->rd/dot_general | solution.py:413
  303.2 0.0 copy-start.2
  303.2 0.0 reduce-scatter.5.cloned.1.call-update
  303.2 43.8 %reduce-scatter.5.cloned.1.call-done = bf16[128,2048]{1,0:T(8,128)(2,1)} async-done(((bf16[512,2048]{1,0:T(8,128)(2,1)}), bf16[128,2048]{1,0:T(8,128)(2,1)}) %reduce-scatter.5.cloned.1.call-update) | async-done | bytes 524304 | tf_op jit(solution)/shard_map/reduce_scatter | solution.py:418
  347.0 0.0 copy-done.2
  347.0 2.1 add_convert_fusion
  (5 shorter events, 0.0 us)
Async XLA Ops:
  6.5 91.9 %copy-start = (bf16[512,2048]{1,0:T(8,128)(2,1)S(1)}, bf16[512,2048]{1,0:T(8,128)(2,1)}, u32[]{:S(2)}) copy-start(bf16[512,2048]{1,0:T(8,128)(2,1)} %param.30) | copy-start | bytes 6291460
  6.5 128.0 %reduce-scatter.3.cloned.1.call-start = ((), (), s32[]{:S(2)}) async-start(), calls=%async_computation.2 | async-start | bytes 2621440 | tf_op jit(solution)/shard_map/reduce_scatter | solution.py:366
  62.8 8.0 %collective-permute-start = (f32[64,512]{1,0:T(8,128)}, f32[64,512]{1,0:T(8,128)S(1)}, u32[]{:S(2)}, u32[]{:S(2)}) collective-permute-start(f32[64,512]{1,0:T(8,128)} %get-tuple-element.11.added_ref), channel_id=1, source_target_pairs={{0,4},{4,8},{8,12},{1,5},{5,9},{9,13},{2,6},{6,10},{10,14},{3,7},{... | collective-permute-start | bytes 393224 | tf_op jit(solution)/shard_map/ppermute | solution.py:305
  73.5 7.1 %collective-permute-start.1 = (f32[64,512]{1,0:T(8,128)}, f32[64,512]{1,0:T(8,128)S(1)}, u32[]{:S(2)}, u32[]{:S(2)}) collective-permute-start(f32[64,512]{1,0:T(8,128)} %advance.2), channel_id=1, source_target_pairs={{0,4},{4,8},{8,12},{1,5},{5,9},{9,13},{2,6},{6,10},{10,14},{3,7},{... | collective-permute-start | bytes 393224 | tf_op jit(solution)/shard_map/ppermute | solution.py:305
  83.2 7.1 %collective-permute-start.2 = (f32[64,512]{1,0:T(8,128)}, f32[64,512]{1,0:T(8,128)S(1)}, u32[]{:S(2)}, u32[]{:S(2)}) collective-permute-start(f32[64,512]{1,0:T(8,128)} %advance.3), channel_id=1, source_target_pairs={{0,4},{4,8},{8,12},{1,5},{5,9},{9,13},{2,6},{6,10},{10,14},{3,7},{... | collective-permute-start | bytes 393224 | tf_op jit(solution)/shard_map/ppermute | solution.py:305
  102.1 0.7 copy-start.4
  102.1 0.7 copy-start.5
  102.1 32.5 %copy-start.1 = (bf16[128,2048]{1,0:T(8,128)(2,1)S(1)}, bf16[128,2048]{1,0:T(8,128)(2,1)}, u32[]{:S(2)}) copy-start(bf16[128,2048]{1,0:T(8,128)(2,1)} %param.31) | copy-start | bytes 1572868
  102.1 33.8 %copy-start.3 = (f32[2048]{0:T(1024)S(1)}, f32[2048]{0:T(1024)}, u32[]{:S(2)}) copy-start(f32[2048]{0:T(1024)} %param.32) | copy-start | bytes 24580
  102.1 83.8 %all-gather.8.cloned.1.call-start = ((), (), s32[]{:S(2)}) async-start(), calls=%async_computation.3 | async-start | bytes 2785280 | tf_op jit(solution)/shard_map/all_gather | solution.py:396
  138.0 82.8 %all-gather.10.cloned.1.call-start = ((), (), s32[]{:S(2)}) async-start(), calls=%async_computation.5 | async-start | bytes 5242880 | tf_op jit(solution)/shard_map/all_gather | solution.py:349
  138.7 118.0 %all-gather.12.cloned.1.call-start = ((), (), s32[]{:S(2)}) async-start(), calls=%async_computation.6 | async-start | bytes 5242880 | tf_op jit(solution)/shard_map/all_gather | solution.py:350
  139.3 153.3 %all-gather.14.cloned.1.call-start = ((), (), s32[]{:S(2)}) async-start(), calls=%async_computation.7 | async-start | bytes 5242880 | tf_op jit(solution)/shard_map/all_gather | solution.py:351
  139.9 207.1 %reduce-scatter.5.cloned.1.call-start = ((), (), s32[]{:S(2)}) async-start(), calls=%async_computation.4 | async-start | bytes 2621440 | tf_op jit(solution)/shard_map/reduce_scatter | solution.py:418
  303.2 43.8 %copy-start.2 = (bf16[128,2048]{1,0:T(8,128)(2,1)S(1)}, bf16[128,2048]{1,0:T(8,128)(2,1)}, u32[]{:S(2)}) copy-start(bf16[128,2048]{1,0:T(8,128)(2,1)} %reduce-scatter.3.cloned.1.call-done) | copy-start | bytes 1572868
Sparse Core Ops, SparseCore 0:
  102.2 32.2 reduce-scatter.2
  138.1 47.7 all-gather.7
  187.5 33.2 all-gather.9
  222.2 34.4 all-gather.11
  258.1 34.4 all-gather.13
  303.3 43.6 reduce-scatter.4

commit v2 on v1

--- a/solution.py
+++ b/solution.py
@@ -311,6 +311,9 @@
         out_specs=by_rows,
         out_shape=jax.ShapeDtypeStruct((length, width), jnp.bfloat16),
         compiler_params=params,
+        cost_estimate=pl.CostEstimate(
+            flops=4_000_000_000, bytes_accessed=20 * length * width, transcendentals=0
+        ),
         name="finish",
     )(
         read_map,
@@ -363,14 +366,11 @@
         self_term_weight,
         lax.axis_size("sp"),
     )
-    proj = lax.psum_scatter(
-        jnp.dot(
-            attention_result, output_weight_matrix, preferred_element_type=jnp.float32
-        ).astype(jnp.bfloat16),
-        "tp",
-        scatter_dimension=0,
-        tiled=True,
-    )
+    part = jnp.dot(
+        attention_result, output_weight_matrix, preferred_element_type=jnp.float32
+    ).astype(jnp.bfloat16)
+    part, gates, ups, downs = lax.optimization_barrier((part, gates, ups, downs))
+    proj = lax.psum_scatter(part, "tp", scatter_dimension=0, tiled=True)
     stream = residual.astype(jnp.float32) + lax.optimization_barrier(proj).astype(jnp.float32)
     ffn_in = (
         stream

time: 357 us -> 269 us (0.75)
  waiting for transfers between devices: 231 us -> 149 us
  matrix products: 20.7 us -> 15.5 us
    all_gather x1, waiting for transfers between devices: 33.6 us -> 0.02 us  [local(): gates = lax.all_gather(gate_weight_experts, 'tp', axis=0)]
    all_gather x1, waiting for transfers between devices: 29.4 us -> 0.02 us  [local(): ups = lax.all_gather(up_weight_experts, 'tp', axis=0)]
    all_gather x1, waiting for transfers between devices: 35.9 us -> 14.7 us  [local(): downs = lax.all_gather(down_weight_experts, 'tp', axis=0)]
    dot_general x1, matrix products: 10.6 us -> 3.79 us  [local(): jnp.einsum('jrf,jfd->rd', hidden, downs[:, own], preferred_element_type=j...]
  transfers between devices with their start and end apart: 9 -> 9, of which waited for: 9 -> 7; matrix products, arithmetic and copies ran while one was open for 2% -> 3% of each run, Pallas kernels for 0% -> 24%
where the time goes in v2:
time: 269 us; the launch traced here: 268 us
  waiting for transfers between devices  149 us (55%)
  Pallas kernels  65.2 us (24%)
  matrix products  15.5 us (6%)
  starting transfers between devices  13.8 us (5%)
  between operations  13.7 us (5%)
  other arithmetic  9.69 us (4%)
    pallas_call x1, Pallas kernels, mixer(): pl.pallas_call(functools.partial(chunk_kernel, head_width), grid=(length...  54.6 us
    all_gather x1, waiting for transfers between devices, local(): lax.all_gather(jnp.concatenate([ffn_in, extra], axis=1), 'sp', axis=0, ti...  47.7 us
    reduce_scatter x1, waiting for transfers between devices, local(): lax.psum_scatter(total.astype(jnp.bfloat16), 'sp', scatter_dimension=0, t...  42.6 us
    reduce_scatter x1, waiting for transfers between devices, local(): proj = lax.psum_scatter(part, 'tp', scatter_dimension=0, tiled=True)  33.3 us
    all_gather x1, waiting for transfers between devices, local(): downs = lax.all_gather(down_weight_experts, 'tp', axis=0)  14.7 us
    ppermute x3, starting transfers between devices, mixer(): got = lax.ppermute(sent, 'sp', [(i, i + 1) for i in range(axis_size - 1)])  13.4 us
    ppermute x3, waiting for transfers between devices, mixer(): got = lax.ppermute(sent, 'sp', [(i, i + 1) for i in range(axis_size - 1)])  8.65 us
    pallas_call x1, Pallas kernels, mixer(): pl.pallas_call(functools.partial(finish_kernel, head_width), grid=(length...  6.63 us
  transfers between devices with their start and end apart: 9, of which 7 were waited for; matrix products, arithmetic and copies ran while one was open for 3% of the time, Pallas kernels for 24%

profile of v2, /device:TPU:0, one launch (start us, length us, event | category | flops | bytes accessed | tf_op | source)
XLA Modules:
  0.0 268.0 jit_solution(940754056100755142)
XLA Ops:
  6.5 0.0 copy-start
  6.5 0.0 copy-start.3
  6.5 0.0 all-gather.10.cloned.1.call-start
  6.5 0.7 all-gather.10.cloned.1.call-update
  7.3 0.0 all-gather.12.cloned.1.call-start
  7.3 0.7 all-gather.12.cloned.1.call-update
  8.0 0.0 all-gather.14.cloned.1.call-start
  8.1 0.7 all-gather.14.cloned.1.call-update
  8.7 0.0 reduce-scatter.3.cloned.1.call-start
  8.8 0.0 copy-done.3
  8.8 0.8 copy.31.offset_ref
  9.6 54.6 %chunks.1 = (f32[512,512]{1,0:T(8,128)}, f32[512,512]{1,0:T(8,128)}, f32[64,512]{1,0:T(8,128)}, f32[64,512]{1,0:T(8,128)}) custom-call(bf16[512,512]{1,0:T(8,128)(2,1)} %recept_ref.3, bf16[512,512]{1,0:T(8,128)(2,1)} %key_ref.3, bf16[512,512]{1,0:T(8,128)(2,1)} %value_ref.3, bf16[512,512]{1,0:T(8,128)(2,1)} %decay_ref.1, bf16[512,512]{1,0:T(8,128)(2,1)} %rate_ref.1, ...), custom_call_target="tpu_custom_call" | custom-call | flops 30000001024 | bytes 2097152 | tf_op jit(solution)/shard_map/chunks/pallas_call | solution.py:275
  64.2 5.0 %collective-permute-start = (f32[64,512]{1,0:T(8,128)}, f32[64,512]{1,0:T(8,128)S(1)}, u32[]{:S(2)}, u32[]{:S(2)}) collective-permute-start(f32[64,512]{1,0:T(8,128)} %get-tuple-element.15.added_ref), channel_id=1, source_target_pairs={{0,4},{4,8},{8,12},{1,5},{5,9},{9,13},{2,6},{6,10},{10,14},{3,7},{... | collective-permute-start | bytes 393224 | tf_op jit(solution)/shard_map/ppermute | solution.py:305
  69.2 3.0 %collective-permute-done = f32[64,512]{1,0:T(8,128)S(1)} collective-permute-done((f32[64,512]{1,0:T(8,128)}, f32[64,512]{1,0:T(8,128)S(1)}, u32[]{:S(2)}, u32[]{:S(2)}) %collective-permute-start) | collective-permute-done | bytes 131104 | tf_op jit(solution)/shard_map/ppermute | solution.py:305
  72.3 0.7 broadcast_select_fusion.state_ref
  72.9 2.0 advance.2
  74.9 4.2 %collective-permute-start.1 = (f32[64,512]{1,0:T(8,128)}, f32[64,512]{1,0:T(8,128)S(1)}, u32[]{:S(2)}, u32[]{:S(2)}) collective-permute-start(f32[64,512]{1,0:T(8,128)} %advance.2), channel_id=1, source_target_pairs={{0,4},{4,8},{8,12},{1,5},{5,9},{9,13},{2,6},{6,10},{10,14},{3,7},{... | collective-permute-start | bytes 393224 | tf_op jit(solution)/shard_map/ppermute | solution.py:305
  79.2 2.8 %collective-permute-done.1 = f32[64,512]{1,0:T(8,128)S(1)} collective-permute-done((f32[64,512]{1,0:T(8,128)}, f32[64,512]{1,0:T(8,128)S(1)}, u32[]{:S(2)}, u32[]{:S(2)}) %collective-permute-start.1) | collective-permute-done | bytes 131104 | tf_op jit(solution)/shard_map/ppermute | solution.py:305
  82.0 0.7 broadcast_select_fusion.1.state_ref
  82.7 2.0 advance.3
  84.6 4.2 %collective-permute-start.2 = (f32[64,512]{1,0:T(8,128)}, f32[64,512]{1,0:T(8,128)S(1)}, u32[]{:S(2)}, u32[]{:S(2)}) collective-permute-start(f32[64,512]{1,0:T(8,128)} %advance.3), channel_id=1, source_target_pairs={{0,4},{4,8},{8,12},{1,5},{5,9},{9,13},{2,6},{6,10},{10,14},{3,7},{... | collective-permute-start | bytes 393224 | tf_op jit(solution)/shard_map/ppermute | solution.py:305
  88.9 2.8 %collective-permute-done.2 = f32[64,512]{1,0:T(8,128)S(1)} collective-permute-done((f32[64,512]{1,0:T(8,128)}, f32[64,512]{1,0:T(8,128)S(1)}, u32[]{:S(2)}, u32[]{:S(2)}) %collective-permute-start.2) | collective-permute-done | bytes 131104 | tf_op jit(solution)/shard_map/ppermute | solution.py:305
  91.7 1.6 broadcast_select_fusion.2.state_ref
  93.3 6.6 %finish.1 = bf16[512,512]{1,0:T(8,128)(2,1)} custom-call(f32[512,512]{1,0:T(8,128)} %get-tuple-element.13.map_ref, f32[512,512]{1,0:T(8,128)} %get-tuple-element.14.own_ref, f32[64,512]{1,0:T(8,128)} %broadcast_select_fusion.2.state_ref, bf16[512,512]{1,0:T(8,128)(2,1)} %recept_ref.3, bf16[512,512]{1,0:T(8,128)(2,1)} %key_ref.3, bf16[512,512]{1,0:T(8,128)(2,1)} %value_ref.3, ...), custom_call_target="tpu_custom_call" | custom-call | flops 4000000000 | bytes 5242880 | tf_op jit(solution)/shard_map/finish/pallas_call | solution.py:307
  99.9 0.0 copy-done
  99.9 3.6 %convolution_convert_fusion = bf16[512,2048]{1,0:T(8,128)(2,1)} fusion(bf16[512,512]{1,0:T(8,128)(2,1)} %finish.1, bf16[512,2048]{1,0:T(8,128)(2,1)S(1)} %copy-done), kind=kOutput, calls=%fused_computation.8 | convolution fusion | flops 1074790400 | bytes 4718592 | tf_op jit(solution)/shard_map/dot_general | solution.py:369
  103.6 0.0 copy-start.6
  103.6 0.0 copy-start.7
  103.6 0.0 copy-start.1
  103.6 0.0 copy-start.4
  103.6 0.0 all-gather.10.cloned.1.call-done
  103.6 0.0 all-gather.12.cloned.1.call-done
  103.6 14.7 %all-gather.14.cloned.1.call-done = bf16[4,256,2048]{2,1,0:T(8,128)(2,1)} async-done(((bf16[1,256,2048]{2,1,0:T(8,128)(2,1)}), bf16[4,256,2048]{2,1,0:T(8,128)(2,1)}) %all-gather.14.cloned.1.call-update) | async-done | bytes 4194320 | tf_op jit(solution)/shard_map/all_gather | solution.py:354
  118.3 0.0 reduce-scatter.3.cloned.1.call-update
  118.3 0.0 all-gather.8.cloned.1.call-start
  118.4 0.0 copy-done.6
  118.4 0.0 copy-done.7
  118.5 0.1 copy.32
  118.6 33.3 %reduce-scatter.3.cloned.1.call-done = bf16[128,2048]{1,0:T(8,128)(2,1)} async-done(((bf16[512,2048]{1,0:T(8,128)(2,1)}), bf16[128,2048]{1,0:T(8,128)(2,1)}) %reduce-scatter.3.cloned.1.call-update) | async-done | bytes 524304 | tf_op jit(solution)/shard_map/reduce_scatter | solution.py:373
  151.9 0.0 copy-done.1
  151.9 1.3 multiply_reduce_fusion
  153.2 0.0 copy-done.4
  153.2 1.3 multiply_convert_fusion
  154.5 0.9 fusion.16
  155.3 0.0 all-gather.8.cloned.1.call-update
  155.3 0.2 reduce-scatter.5.cloned.1.call-start
  155.6 47.7 %all-gather.8.cloned.1.call-done = bf16[512,2176]{1,0:T(8,128)(2,1)} async-done(((bf16[128,2176]{1,0:T(8,128)(2,1)}), bf16[512,2176]{1,0:T(8,128)(2,1)}) %all-gather.8.cloned.1.call-update) | async-done | bytes 2228240 | tf_op jit(solution)/shard_map/all_gather | solution.py:396
  203.3 0.9 slice_convert_fusion
  204.3 0.3 fusion.18
  204.6 0.0 copy-start.5
  204.6 0.0 copy-start.8
  204.6 5.4 %fusion.5 = f32[4,256,512]{2,1,0:T(8,128)S(1)} fusion(bf16[4,1,2048,256]{3,2,0,1:T(8,128)(2,1)} %bitcast.48, bf16[512,2176]{1,0:T(8,128)(2,1)} %all-gather.8.cloned.1.call-done), kind=kOutput, calls=%fused_computation.6 | convolution fusion | flops 2147483648 | bytes 8388608 | tf_op jit(solution)/shard_map/rd,jdf->jrf/dot_general | solution.py:406
  210.0 0.0 copy-done.5
  210.0 0.0 copy-done.8
  210.0 0.0 copy-start.9
  210.0 2.7 fusion.9
  212.7 0.0 copy-done.9
  212.7 3.8 %fusion = bf16[512,2048]{1,0:T(8,128)(2,1)} fusion(bf16[4,512,256]{1,2,0:T(8,128)(2,1)S(1)} %fusion.9, bf16[4,1,256,2048]{3,2,0,1:T(8,128)(2,1)S(1)} %bitcast.50, f32[512]{0:T(512)S(1)} %fusion.18), kind=kOutput, calls=%fused_computation.1 | convolution fusion | flops 2149580800 | bytes 7342080 | tf_op jit(solution)/shard_map/jrf,jfd->rd/dot_general | solution.py:413
  216.5 0.0 copy-start.2
  216.5 0.0 reduce-scatter.5.cloned.1.call-update
  216.5 42.6 %reduce-scatter.5.cloned.1.call-done = bf16[128,2048]{1,0:T(8,128)(2,1)} async-done(((bf16[512,2048]{1,0:T(8,128)(2,1)}), bf16[128,2048]{1,0:T(8,128)(2,1)}) %reduce-scatter.5.cloned.1.call-update) | async-done | bytes 524304 | tf_op jit(solution)/shard_map/reduce_scatter | solution.py:418
  259.0 0.0 copy-done.2
  259.0 2.1 add_convert_fusion
  (5 shorter events, 0.0 us)
Async XLA Ops:
  6.5 93.4 %copy-start = (bf16[512,2048]{1,0:T(8,128)(2,1)S(1)}, bf16[512,2048]{1,0:T(8,128)(2,1)}, u32[]{:S(2)}) copy-start(bf16[512,2048]{1,0:T(8,128)(2,1)} %param.30) | copy-start | bytes 6291460
  6.5 2.3 copy-start.3
  6.5 97.1 %all-gather.10.cloned.1.call-start = ((), (), s32[]{:S(2)}) async-start(), calls=%async_computation.5 | async-start | bytes 5242880 | tf_op jit(solution)/shard_map/all_gather | solution.py:352
  7.3 96.4 %all-gather.12.cloned.1.call-start = ((), (), s32[]{:S(2)}) async-start(), calls=%async_computation.6 | async-start | bytes 5242880 | tf_op jit(solution)/shard_map/all_gather | solution.py:353
  8.0 110.3 %all-gather.14.cloned.1.call-start = ((), (), s32[]{:S(2)}) async-start(), calls=%async_computation.7 | async-start | bytes 5242880 | tf_op jit(solution)/shard_map/all_gather | solution.py:354
  8.7 143.1 %reduce-scatter.3.cloned.1.call-start = ((), (), s32[]{:S(2)}) async-start(), calls=%async_computation.2 | async-start | bytes 2621440 | tf_op jit(solution)/shard_map/reduce_scatter | solution.py:373
  64.2 8.0 %collective-permute-start = (f32[64,512]{1,0:T(8,128)}, f32[64,512]{1,0:T(8,128)S(1)}, u32[]{:S(2)}, u32[]{:S(2)}) collective-permute-start(f32[64,512]{1,0:T(8,128)} %get-tuple-element.15.added_ref), channel_id=1, source_target_pairs={{0,4},{4,8},{8,12},{1,5},{5,9},{9,13},{2,6},{6,10},{10,14},{3,7},{... | collective-permute-start | bytes 393224 | tf_op jit(solution)/shard_map/ppermute | solution.py:305
  74.9 7.1 %collective-permute-start.1 = (f32[64,512]{1,0:T(8,128)}, f32[64,512]{1,0:T(8,128)S(1)}, u32[]{:S(2)}, u32[]{:S(2)}) collective-permute-start(f32[64,512]{1,0:T(8,128)} %advance.2), channel_id=1, source_target_pairs={{0,4},{4,8},{8,12},{1,5},{5,9},{9,13},{2,6},{6,10},{10,14},{3,7},{... | collective-permute-start | bytes 393224 | tf_op jit(solution)/shard_map/ppermute | solution.py:305
  84.6 7.1 %collective-permute-start.2 = (f32[64,512]{1,0:T(8,128)}, f32[64,512]{1,0:T(8,128)S(1)}, u32[]{:S(2)}, u32[]{:S(2)}) collective-permute-start(f32[64,512]{1,0:T(8,128)} %advance.3), channel_id=1, source_target_pairs={{0,4},{4,8},{8,12},{1,5},{5,9},{9,13},{2,6},{6,10},{10,14},{3,7},{... | collective-permute-start | bytes 393224 | tf_op jit(solution)/shard_map/ppermute | solution.py:305
  103.6 14.8 %copy-start.6 = (f32[128,2]{0,1:T(2,128)S(1)}, f32[128,2]{0,1:T(2,128)}, u32[]{:S(2)}) copy-start(f32[128,2]{0,1:T(2,128)} %param.34) | copy-start | bytes 3076
  103.6 14.8 %copy-start.7 = (s32[128,2]{0,1:T(2,128)S(1)}, s32[128,2]{0,1:T(2,128)}, u32[]{:S(2)}) copy-start(s32[128,2]{0,1:T(2,128)} %param.33) | copy-start | bytes 3076
  103.6 48.3 %copy-start.1 = (bf16[128,2048]{1,0:T(8,128)(2,1)S(1)}, bf16[128,2048]{1,0:T(8,128)(2,1)}, u32[]{:S(2)}) copy-start(bf16[128,2048]{1,0:T(8,128)(2,1)} %param.31) | copy-start | bytes 1572868
  103.6 49.6 %copy-start.4 = (f32[2048]{0:T(1024)S(1)}, f32[2048]{0:T(1024)}, u32[]{:S(2)}) copy-start(f32[2048]{0:T(1024)} %param.32) | copy-start | bytes 24580
  118.3 85.0 %all-gather.8.cloned.1.call-start = ((), (), s32[]{:S(2)}) async-start(), calls=%async_computation.3 | async-start | bytes 2785280 | tf_op jit(solution)/shard_map/all_gather | solution.py:396
  155.3 103.7 %reduce-scatter.5.cloned.1.call-start = ((), (), s32[]{:S(2)}) async-start(), calls=%async_computation.4 | async-start | bytes 2621440 | tf_op jit(solution)/shard_map/reduce_scatter | solution.py:418
  204.6 5.4 %copy-start.5 = (bf16[512,2176]{1,0:T(8,128)(2,1)S(1)}, bf16[512,2176]{1,0:T(8,128)(2,1)}, u32[]{:S(2)}) copy-start(bf16[512,2176]{1,0:T(8,128)(2,1)} %all-gather.8.cloned.1.call-done) | copy-start | bytes 6684676
  204.6 5.4 %copy-start.8 = (bf16[4,2048,256]{2,1,0:T(8,128)(2,1)S(1)}, bf16[4,2048,256]{2,1,0:T(8,128)(2,1)}, u32[]{:S(2)}) copy-start(bf16[4,2048,256]{2,1,0:T(8,128)(2,1)} %all-gather.12.cloned.1.call-done) | copy-start | bytes 12582916
  210.0 2.7 %copy-start.9 = (bf16[4,256,2048]{2,1,0:T(8,128)(2,1)S(1)}, bf16[4,256,2048]{2,1,0:T(8,128)(2,1)}, u32[]{:S(2)}) copy-start(bf16[4,256,2048]{2,1,0:T(8,128)(2,1)} %all-gather.14.cloned.1.call-done) | copy-start | bytes 12582916
  216.5 42.6 %copy-start.2 = (bf16[128,2048]{1,0:T(8,128)(2,1)S(1)}, bf16[128,2048]{1,0:T(8,128)(2,1)}, u32[]{:S(2)}) copy-start(bf16[128,2048]{1,0:T(8,128)(2,1)} %reduce-scatter.3.cloned.1.call-done) | copy-start | bytes 1572868
Sparse Core Ops, SparseCore 0:
  8.9 37.3 all-gather.9
  47.8 34.3 all-gather.11
  83.8 34.4 all-gather.13
  120.7 31.1 reduce-scatter.2
  155.5 47.8 all-gather.7
  216.6 42.3 reduce-scatter.4
